TPU v7x, 32 devices: a whole 2x2x4 slice. The times are simulated.
32 devices in a mesh: fs: 8 (over z, x), tp: 4 (over y, core).
Axes of the slice: x: 2, y: 2, z: 4, core: 2. Of those that a mesh axis runs over, the one named last changes fastest.
Arguments:
- tokens: bfloat16 [8192, 2048], P('fs'), may hold values from -3 to 3
- gate_weight: bfloat16 [2048, 5632], P('fs', 'tp'), may hold values from -0.125 to 0.125
- value_weight: bfloat16 [2048, 5632], P('fs', 'tp'), may hold values from -0.125 to 0.125
- gate_taps: bfloat16 [3, 5632], P(None, 'tp'), may hold values from -3 to 3
- value_taps: bfloat16 [3, 5632], P(None, 'tp'), may hold values from -3 to 3
- down_weight: bfloat16 [5632, 2048], P('tp', 'fs'), may hold values from -0.078125 to 0.078125
- norm_gain: float32 [2048], replicated, may hold values from 0.1 to 1.9
- norm_bias: float32 [2048], replicated, may hold values from -3 to 3
Outputs:
- normed: bfloat16 [8192, 2048], P('fs')
All inputs are finite; a program needn't handle non-finite values.
Results may differ from a plain program's by a relative error of at most 0.005.
Values may be sent and summed in bfloat16 or wider, within the bound.
A program may use at most 64 MiB of HBM per device.

v0:
```python
import jax
import jax.numpy as jnp
from jax import lax
from jax.sharding import PartitionSpec as P

EPSILON = 1e-05
RESIDUAL_SCALE = 8.0**0.25


def rounded(values):
    return lax.optimization_barrier(values.astype(jnp.bfloat16)).astype(jnp.float32)


def centred_conv(values, taps):
    padded = jnp.pad(values, ((1, 1), (0, 0)))
    return padded[:-2] * taps[0] + padded[1:-1] * taps[1] + padded[2:] * taps[2]


def finish(summed, residual, norm_gain, norm_bias):
    mixed = RESIDUAL_SCALE * residual.astype(jnp.float32) + rounded(summed)
    centered = mixed - jnp.mean(mixed, -1, keepdims=True)
    variance = jnp.mean(centered * centered, -1, keepdims=True)
    normed = centered * lax.rsqrt(variance + EPSILON) * norm_gain + norm_bias
    return normed.astype(jnp.bfloat16)


def on_device(
    tokens, gate_weight, value_weight, gate_taps, value_taps, down_weight, norm_gain, norm_bias
):

    def add_rows(portion):
        return jnp.dot(tokens, portion, preferred_element_type=jnp.float32)

    gate_sum = add_rows(lax.all_gather(gate_weight, "fs", axis=0, tiled=True))
    value_sum = add_rows(lax.all_gather(value_weight, "fs", axis=0, tiled=True))
    gate_conv = centred_conv(rounded(gate_sum), gate_taps.astype(jnp.float32))
    value_conv = centred_conv(rounded(value_sum), value_taps.astype(jnp.float32))
    hidden = (jax.nn.silu(gate_conv) * value_conv).astype(jnp.bfloat16)
    partials = rounded(
        jnp.dot(
            hidden,
            lax.all_gather(down_weight, "fs", axis=1, tiled=True),
            preferred_element_type=jnp.float32,
        )
    )
    shares = lax.psum_scatter(
        partials.astype(jnp.bfloat16), "tp", scatter_dimension=0, tiled=True
    ).astype(jnp.float32)
    share_rows = shares.shape[0]
    own_rows = lax.dynamic_slice_in_dim(tokens, lax.axis_index("tp") * share_rows, share_rows, 0)
    normed_share = finish(shares, own_rows, norm_gain, norm_bias)
    return lax.all_gather(normed_share, "tp", axis=0, tiled=True)


def solution(mesh):
    in_specs = (
        P("fs", None),
        P("fs", "tp"),
        P("fs", "tp"),
        P(None, "tp"),
        P(None, "tp"),
        P("tp", "fs"),
        P(),
        P(),
    )
    out_specs = P("fs", None)
    return jax.shard_map(
        on_device, mesh=mesh, in_specs=in_specs, out_specs=out_specs, check_vma=False
    )
```

profile of v0, /device:TPU:0, one launch (start us, length us, event | category | flops | bytes accessed | tf_op | source)
XLA Modules:
  0.0 410.2 jit_solution(2290608909475831313)
XLA Ops:
  6.5 0.0 all-gather.5.cloned.1.call-start
  6.5 0.7 all-gather.5.cloned.1.call-update
  7.3 0.0 all-gather.7.cloned.1.call-start
  7.3 0.7 all-gather.7.cloned.1.call-update
  8.0 0.0 all-gather.9.cloned.1.call-start
  8.1 0.7 all-gather.9.cloned.1.call-update
  8.7 0.0 reduce-scatter.2.cloned.1.call-start
  8.8 0.7 convert_element_type.43
  9.5 0.7 convert_element_type.46
  10.2 0.1 slice_reduce_fusion.2
  10.3 94.3 %all-gather.5.cloned.1.call-done = bf16[2048,1408]{1,0:T(8,128)(2,1)} async-done(((bf16[256,1408]{1,0:T(8,128)(2,1)}), bf16[2048,1408]{1,0:T(8,128)(2,1)}) %all-gather.5.cloned.1.call-update) | async-done | bytes 5767184 | tf_op jit(solution)/shard_map/all_gather | solution.py:34
  104.6 10.1 %convolution_convert_fusion.1 = bf16[1024,1408]{1,0:T(8,128)(2,1)S(1)} fusion(bf16[1024,2048]{1,0:T(8,128)(2,1)} %param.8, bf16[2048,1408]{1,0:T(8,128)(2,1)} %all-gather.5.cloned.1.call-done), kind=kOutput, calls=%fused_computation.2 | convolution fusion | flops 5907021824 | bytes 12845056 | tf_op jit(solution)/shard_map/dot_general | solution.py:32
  114.7 2.8 convert_element_type.42
  117.5 79.8 %all-gather.7.cloned.1.call-done = bf16[2048,1408]{1,0:T(8,128)(2,1)} async-done(((bf16[256,1408]{1,0:T(8,128)(2,1)}), bf16[2048,1408]{1,0:T(8,128)(2,1)}) %all-gather.7.cloned.1.call-update) | async-done | bytes 5767184 | tf_op jit(solution)/shard_map/all_gather | solution.py:35
  197.3 10.1 %convolution_convert_fusion = bf16[1024,1408]{1,0:T(8,128)(2,1)S(1)} fusion(bf16[1024,2048]{1,0:T(8,128)(2,1)} %param.8, bf16[2048,1408]{1,0:T(8,128)(2,1)} %all-gather.7.cloned.1.call-done), kind=kOutput, calls=%fused_computation.1 | convolution fusion | flops 5907021824 | bytes 12845056 | tf_op jit(solution)/shard_map/dot_general | solution.py:32
  207.4 2.9 convert_element_type.45
  210.3 80.3 %all-gather.9.cloned.1.call-done = bf16[1408,2048]{1,0:T(8,128)(2,1)} async-done(((bf16[1408,256]{1,0:T(8,128)(2,1)}), bf16[1408,2048]{1,0:T(8,128)(2,1)}) %all-gather.9.cloned.1.call-update) | async-done | bytes 5767184 | tf_op jit(solution)/shard_map/all_gather | solution.py:42
  290.7 23.4 %convolution_convert_fusion.2 = bf16[1024,2048]{1,0:T(8,128)(2,1)} fusion(bf16[1408,2048]{1,0:T(8,128)(2,1)} %all-gather.9.cloned.1.call-done, f32[1024,1408]{1,0:T(8,128)} %convert_element_type.45, f32[1024,1408]{1,0:T(8,128)} %convert_element_type.42, f32[1408]{0:T(1024)S(1)} %get-tuple-element.9, f32[1408]{0:T(1024)S(1)} %get-tuple-element.10, ...), kind=kOutput, calls=%fused_computation.3 | convolution fusion | flops 5930745856 | bytes 21529600 | tf_op jit(solution)/shard_map/dot_general | solution.py:40
  314.1 0.0 copy-start
  314.1 0.0 copy-start.1
  314.1 0.0 reduce-scatter.2.cloned.1.call-update
  314.2 0.0 all-gather.11.cloned.1.call-start
  314.2 42.9 %reduce-scatter.2.cloned.1.call-done = bf16[256,2048]{1,0:T(8,128)(2,1)} async-done(((bf16[1024,2048]{1,0:T(8,128)(2,1)}), bf16[256,2048]{1,0:T(8,128)(2,1)}) %reduce-scatter.2.cloned.1.call-update) | async-done | bytes 1048592 | tf_op jit(solution)/shard_map/reduce_scatter | solution.py:46
  357.1 2.0 fusion
  359.0 2.1 multiply_reduce_fusion
  361.1 0.0 copy-done
  361.1 0.0 copy-done.1
  361.2 3.1 add_convert_fusion
  364.3 0.0 all-gather.11.cloned.1.call-update
  364.3 34.6 %all-gather.11.cloned.1.call-done = bf16[1024,2048]{1,0:T(8,128)(2,1)} async-done(((bf16[256,2048]{1,0:T(8,128)(2,1)}), bf16[1024,2048]{1,0:T(8,128)(2,1)}) %all-gather.11.cloned.1.call-update) | async-done | bytes 4194320 | tf_op jit(solution)/shard_map/all_gather | solution.py:52
  398.9 4.8 %copy.10 = bf16[1024,2048]{1,0:T(8,128)(2,1)} copy(bf16[1024,2048]{1,0:T(8,128)(2,1)} %all-gather.11.cloned.1.call-done) | data formatting | bytes 8388608
  (2 shorter events, 0.0 us)
Async XLA Ops:
  6.5 98.0 %all-gather.5.cloned.1.call-start = ((), (), s32[]{:S(2)}) async-start(), calls=%async_computation.1 | async-start | bytes 6488064 | tf_op jit(solution)/shard_map/all_gather | solution.py:34
  7.3 190.0 %all-gather.7.cloned.1.call-start = ((), (), s32[]{:S(2)}) async-start(), calls=%async_computation.2 | async-start | bytes 6488064 | tf_op jit(solution)/shard_map/all_gather | solution.py:35
  8.0 282.7 %all-gather.9.cloned.1.call-start = ((), (), s32[]{:S(2)}) async-start(), calls=%async_computation.3 | async-start | bytes 6488064 | tf_op jit(solution)/shard_map/all_gather | solution.py:42
  8.7 348.3 %reduce-scatter.2.cloned.1.call-start = ((), (), s32[]{:S(2)}) async-start(), calls=%async_computation.4 | async-start | bytes 5242880 | tf_op jit(solution)/shard_map/reduce_scatter | solution.py:46
  314.1 47.0 %copy-start = (f32[2048]{0:T(1024)S(1)}, f32[2048]{0:T(1024)}, u32[]{:S(2)}) copy-start(f32[2048]{0:T(1024)} %param.15) | copy-start | bytes 24580
  314.1 47.0 %copy-start.1 = (f32[2048]{0:T(1024)S(1)}, f32[2048]{0:T(1024)}, u32[]{:S(2)}) copy-start(f32[2048]{0:T(1024)} %param.14) | copy-start | bytes 24580
  314.2 84.8 %all-gather.11.cloned.1.call-start = ((), (), s32[]{:S(2)}) async-start(), calls=%async_computation.5 | async-start | bytes 5242880 | tf_op jit(solution)/shard_map/all_gather | solution.py:52
Sparse Core Ops, SparseCore 0:
  9.5 95.0 all-gather.4
  106.8 90.4 all-gather.6
  199.3 91.3 all-gather.8
  314.3 42.7 reduce-scatter.1
  364.4 34.4 all-gather.10
where the time goes:
time: 411 us; the launch traced here: 410 us
  waiting for transfers between devices  334 us (81%)
  matrix products  43.7 us (11%)
  other arithmetic  14.4 us (4%)
  between operations  13.2 us (3%)
  local copies, waits for them, and re-layouts  4.88 us (1%)
    all_gather x1, waiting for transfers between devices, on_device(): gate_sum = add_rows(lax.all_gather(gate_weight, 'fs', axis=0, tiled=True))  94.3 us
    all_gather x1, waiting for transfers between devices, on_device(): lax.all_gather(down_weight, 'fs', axis=1, tiled=True)  80.3 us
    all_gather x1, waiting for transfers between devices, on_device(): value_sum = add_rows(lax.all_gather(value_weight, 'fs', axis=0, tiled=True))  79.8 us
    reduce_scatter x1, waiting for transfers between devices, on_device(): lax.psum_scatter(partials.astype(jnp.bfloat16), 'tp', scatter_dimension=0...  42.9 us
    all_gather x1, waiting for transfers between devices, on_device(): return lax.all_gather(normed_share, 'tp', axis=0, tiled=True)  34.6 us
    dot_general x1, matrix products, on_device(): jnp.dot(hidden, lax.all_gather(down_weight, 'fs', axis=1, tiled=True), pr...  23.4 us
    dot_general x2, matrix products, add_rows(): return jnp.dot(tokens, portion, preferred_element_type=jnp.float32)  20.2 us
  transfers between devices with their start and end apart: 5, of which 5 were waited for; matrix products, arithmetic and copies ran while one was open for 7% of the time, Pallas kernels for 0%

commit v1 on v0

--- a/solution.py
+++ b/solution.py
@@ -1,10 +1,16 @@
+import functools
+
 import jax
 import jax.numpy as jnp
 from jax import lax
+from jax.experimental import pallas as pl
+from jax.experimental.pallas import tpu as pltpu
 from jax.sharding import PartitionSpec as P
 
 EPSILON = 1e-05
 RESIDUAL_SCALE = 8.0**0.25
+LANES = 128
+VMEM_BYTES = 67043328
 
 
 def rounded(values):
@@ -24,10 +30,9 @@
     return normed.astype(jnp.bfloat16)
 
 
-def on_device(
+def collective_form(
     tokens, gate_weight, value_weight, gate_taps, value_taps, down_weight, norm_gain, norm_bias
 ):
-
     def add_rows(portion):
         return jnp.dot(tokens, portion, preferred_element_type=jnp.float32)
 
@@ -52,18 +57,304 @@
     return lax.all_gather(normed_share, "tp", axis=0, tiled=True)
 
 
+def branch_kernel(
+    n, t_ref, g_ref, v_ref, gt_ref, vt_ref, d_ref, out_ref,
+    gbuf, vbuf, dbuf, acc_g, acc_v, hid, pbuf, rbuf, cbuf, ybuf, obuf,
+    w_send, w_recv, c_send, c_recv, y_send, y_recv, o_send, o_recv,
+):
+    rows, units = hid.shape
+    half_rows = rows // 2
+    tile = 256
+    fs = lax.axis_index("fs")
+    tp = lax.axis_index("tp")
+    core = lax.rem(tp, 2)
+    partner = tp + 1 - 2 * core
+    across = lax.rem(tp + 2, 4)
+    half_n = n // 2
+
+    x, z = lax.rem(fs, 2), lax.div(fs, 2)
+    pos = (1 - x) * z + x * (n - 1 - z)
+
+    def at_pos(p):
+        p = lax.rem(p, n)
+        down = lax.div(p, half_n)
+        return (1 - down) * 2 * p + down * (2 * (n - 1 - p) + 1)
+
+    right, left = at_pos(pos + 1), at_pos(pos + n - 1)
+
+    barrier = pltpu.get_barrier_semaphore()
+    for target in ({"fs": left}, {"fs": right}, {"tp": partner}, {"tp": across}):
+        pl.semaphore_signal(
+            barrier, inc=1, device_id=target, device_id_type=pl.DeviceIdType.MESH
+        )
+    pl.semaphore_wait(barrier, 4)
+
+    streams = ((g_ref, gbuf), (v_ref, vbuf), (d_ref, dbuf))
+
+    def hop(stream, way, step, first=False):
+        own, slots = streams[stream]
+        part = pl.ds(way * LANES, LANES)
+        where = (slice(None), part) if stream == 2 else (part, slice(None))
+        source = own.at[where] if first else slots.at[(step - 1,) + where]
+        k = stream * 2 + way
+        return pltpu.make_async_remote_copy(
+            src_ref=source,
+            dst_ref=slots.at[(step,) + where],
+            send_sem=w_send.at[k, step],
+            recv_sem=w_recv.at[k, step],
+            device_id={"fs": right if way == 0 else left},
+            device_id_type=pl.DeviceIdType.MESH,
+        )
+
+    def begin(stream):
+        for way in range(2):
+            hop(stream, way, 0, True).start()
+
+    def arrive(stream, step):
+        for way in range(2):
+            hop(stream, way, step - 1, True).wait_recv()
+
+            @pl.when(step < n - 1)
+            def _():
+                hop(stream, way, step).start()
+
+    begin(0)
+    begin(1)
+
+    def token_tile(r, step):
+        row = pl.ds(pl.multiple_of(r * tile, tile), tile)
+        a = pl.multiple_of(at_pos(pos + n - step) * 2 * LANES, LANES)
+        b = pl.multiple_of(at_pos(pos + step) * 2 * LANES + LANES, LANES)
+        return row, jnp.concatenate(
+            [t_ref[row, pl.ds(a, LANES)], t_ref[row, pl.ds(b, LANES)]], axis=1
+        )
+
+    @pl.loop(0, rows // tile)
+    def _(r):
+        row, lhs = token_tile(r, 0)
+        acc_g[row, :] = jnp.dot(lhs, g_ref[...], preferred_element_type=jnp.float32)
+        acc_v[row, :] = jnp.dot(lhs, v_ref[...], preferred_element_type=jnp.float32)
+
+    @pl.loop(1, n)
+    def _(step):
+        @pl.when(step == n - 1)
+        def _():
+            arrive(2, 1)
+
+        arrive(0, step)
+        arrive(1, step)
+
+        @pl.when(step == n - 3)
+        def _():
+            begin(2)
+
+        @pl.loop(0, rows // tile)
+        def _(r):
+            row, lhs = token_tile(r, step)
+            acc_g[row, :] += jnp.dot(lhs, gbuf[step - 1], preferred_element_type=jnp.float32)
+            acc_v[row, :] += jnp.dot(lhs, vbuf[step - 1], preferred_element_type=jnp.float32)
+
+    row_id = lax.broadcasted_iota(jnp.int32, (rows, LANES), 0)
+
+    def conv(acc, taps, cols):
+        v = acc[:, cols].astype(jnp.bfloat16).astype(jnp.float32)
+        c = taps[:, cols].astype(jnp.float32)
+        before = jnp.where(row_id == 0, 0.0, pltpu.roll(v, 1, 0))
+        after = jnp.where(row_id == rows - 1, 0.0, pltpu.roll(v, rows - 1, 0))
+        return before * c[0:1] + v * c[1:2] + after * c[2:3]
+
+    chunks = units // LANES
+
+    @pl.loop(0, chunks)
+    def _(i):
+        cols = pl.ds(pl.multiple_of(i * LANES, LANES), LANES)
+        gate = conv(acc_g, gt_ref, cols)
+        value = conv(acc_v, vt_ref, cols)
+        hid[:, cols] = (gate / (1.0 + jnp.exp(-gate)) * value).astype(jnp.bfloat16)
+
+        @pl.when(i == chunks // 2)
+        def _():
+            arrive(2, 2)
+
+    mine = pl.ds(pl.multiple_of(core * half_rows, half_rows), half_rows)
+    other = pl.ds(pl.multiple_of((1 - core) * half_rows, half_rows), half_rows)
+
+    def to_partner(step):
+        return pltpu.make_async_remote_copy(
+            src_ref=pbuf.at[step, other],
+            dst_ref=rbuf.at[step],
+            send_sem=c_send.at[step],
+            recv_sem=c_recv.at[step],
+            device_id={"tp": partner},
+            device_id_type=pl.DeviceIdType.MESH,
+        )
+
+    def to_across(step):
+        return pltpu.make_async_remote_copy(
+            src_ref=cbuf.at[step],
+            dst_ref=ybuf.at[step],
+            send_sem=y_send.at[step],
+            recv_sem=y_recv.at[step],
+            device_id={"tp": across},
+            device_id_type=pl.DeviceIdType.MESH,
+        )
+
+    def out_cols(step, way):
+        owner = at_pos(pos + n - step) if way == 0 else at_pos(pos + step)
+        return pl.ds(pl.multiple_of(owner * 2 * LANES + way * LANES, LANES), LANES)
+
+    def to_out(step, way, where):
+        cols = out_cols(step, way)
+        return pltpu.make_async_remote_copy(
+            src_ref=obuf.at[step, :, pl.ds(way * LANES, LANES)],
+            dst_ref=out_ref.at[where, cols],
+            send_sem=o_send.at[way, step],
+            recv_sem=o_recv.at[way, step],
+            device_id={"tp": partner},
+            device_id_type=pl.DeviceIdType.MESH,
+        )
+
+    def project(step, weight):
+        @pl.loop(0, rows // tile)
+        def _(r):
+            row = pl.ds(pl.multiple_of(r * tile, tile), tile)
+            pbuf[step, row, :] = jnp.dot(
+                hid[row, :], weight, preferred_element_type=jnp.float32
+            ).astype(jnp.bfloat16)
+
+        to_partner(step).start()
+        to_partner(step).wait_recv()
+        cbuf[step] = (
+            pbuf[step, mine].astype(jnp.float32) + rbuf[step].astype(jnp.float32)
+        ).astype(jnp.bfloat16)
+        to_across(step).start()
+
+    def settle(step):
+        to_across(step).wait_recv()
+        total = (
+            cbuf[step].astype(jnp.float32) + ybuf[step].astype(jnp.float32)
+        ).astype(jnp.bfloat16)
+        obuf[step] = total
+        for way in range(2):
+            to_out(step, way, mine).start()
+            out_ref[mine, out_cols(step, way)] = total[:, way * LANES:(way + 1) * LANES]
+
+    project(0, d_ref[...])
+
+    @pl.loop(1, n)
+    def _(step):
+        @pl.when(step > 2)
+        def _():
+            arrive(2, step)
+
+        project(step, dbuf[step - 1])
+
+        @pl.when(step >= 2)
+        def _():
+            settle(step - 2)
+
+    settle(n - 2)
+    settle(n - 1)
+
+    @pl.loop(0, n - 1)
+    def _(step):
+        for stream in range(3):
+            for way in range(2):
+                hop(stream, way, step, True).wait_send()
+
+    @pl.loop(0, n)
+    def _(step):
+        to_partner(step).wait_send()
+        to_across(step).wait_send()
+        for way in range(2):
+            to_out(step, way, mine).wait_send()
+            to_out(step, way, other).wait_recv()
+
+
+def norm_kernel(b_ref, t_ref, gain_ref, bias_ref, out_ref):
+    mixed = RESIDUAL_SCALE * t_ref[...].astype(jnp.float32) + b_ref[...].astype(jnp.float32)
+    centered = mixed - jnp.mean(mixed, -1, keepdims=True)
+    variance = jnp.mean(centered * centered, -1, keepdims=True)
+    normed = centered * lax.rsqrt(variance + EPSILON) * gain_ref[...] + bias_ref[...]
+    out_ref[...] = normed.astype(jnp.bfloat16)
+
+
+def kernel_form(
+    n, tokens, gate_weight, value_weight, gate_taps, value_taps, down_weight, norm_gain, norm_bias
+):
+    rows, width = tokens.shape
+    depth, units = gate_weight.shape
+    bf16, f32 = jnp.bfloat16, jnp.float32
+    dma = pltpu.SemaphoreType.DMA
+    branch = pl.pallas_call(
+        functools.partial(branch_kernel, n),
+        out_shape=jax.ShapeDtypeStruct((rows, width), bf16),
+        in_specs=[pl.BlockSpec(memory_space=pltpu.VMEM)] * 6,
+        out_specs=pl.BlockSpec(memory_space=pltpu.VMEM),
+        scratch_shapes=[
+            pltpu.VMEM((n - 1, depth, units), bf16),
+            pltpu.VMEM((n - 1, depth, units), bf16),
+            pltpu.VMEM((n - 1, units, depth), bf16),
+            pltpu.VMEM((rows, units), f32),
+            pltpu.VMEM((rows, units), f32),
+            pltpu.VMEM((rows, units), bf16),
+            pltpu.VMEM((n, rows, depth), bf16),
+            pltpu.VMEM((n, rows // 2, depth), bf16),
+            pltpu.VMEM((n, rows // 2, depth), bf16),
+            pltpu.VMEM((n, rows // 2, depth), bf16),
+            pltpu.VMEM((n, rows // 2, depth), bf16),
+            dma((6, n - 1)),
+            dma((6, n - 1)),
+            dma((n,)),
+            dma((n,)),
+            dma((n,)),
+            dma((n,)),
+            dma((2, n)),
+            dma((2, n)),
+        ],
+        compiler_params=pltpu.CompilerParams(
+            collective_id=0, has_side_effects=True, vmem_limit_bytes=VMEM_BYTES
+        ),
+        name="branch",
+    )(tokens, gate_weight, value_weight, gate_taps, value_taps, down_weight)
+    block = 256
+    by_rows = pl.BlockSpec((block, width), lambda i: (i, 0))
+    whole = pl.BlockSpec((1, width), lambda i: (0, 0))
+    return pl.pallas_call(
+        norm_kernel,
+        grid=(rows // block,),
+        out_shape=jax.ShapeDtypeStruct((rows, width), bf16),
+        in_specs=[by_rows, by_rows, whole, whole],
+        out_specs=by_rows,
+        name="norm",
+    )(branch, tokens, norm_gain.reshape(1, width), norm_bias.reshape(1, width))
+
+
 def solution(mesh):
-    in_specs = (
-        P("fs", None),
-        P("fs", "tp"),
-        P("fs", "tp"),
-        P(None, "tp"),
-        P(None, "tp"),
-        P("tp", "fs"),
-        P(),
-        P(),
+    n_fs, n_tp = mesh.shape["fs"], mesh.shape["tp"]
+
+    def on_device(tokens, gate_weight, *rest):
+        rows = tokens.shape[0]
+        depth, units = gate_weight.shape
+        fits = n_tp == 4 and n_fs % 2 == 0 and n_fs >= 6
+        fits = fits and depth == 2 * LANES and units % LANES == 0 and rows % 512 == 0
+        if fits:
+            return kernel_form(n_fs, tokens, gate_weight, *rest)
+        return collective_form(tokens, gate_weight, *rest)
+
+    return jax.shard_map(
+        on_device,
+        mesh=mesh,
+        in_specs=(
+            P("fs", None),
+            P("fs", "tp"),
+            P("fs", "tp"),
+            P(None, "tp"),
+            P(None, "tp"),
+            P("tp", "fs"),
+            P(None),
+            P(None),
+        ),
+        out_specs=P("fs", None),
+        check_vma=False,
     )
-    out_specs = P("fs", None)
-    return jax.shard_map(
-        on_device, mesh=mesh, in_specs=in_specs, out_specs=out_specs, check_vma=False
-    )

time: 411 us -> 205 us (0.50)
  waiting for transfers between devices: 334 us -> 0 us
  Pallas kernels: 0 us -> 205 us
  matrix products: 43.7 us -> 0 us
  other arithmetic: 14.4 us -> 0 us
  between operations: 13.2 us -> 0.01 us
  local copies, waits for them, and re-layouts: 4.88 us -> 0 us
    all_gather x4 -> x0, waiting for transfers between devices: 289 us -> none  [the longest x1 94.3 us: on_device(): gate_sum = add_rows(lax.all_gather(gate_weight, 'fs', axis=0, tiled=True))]
    pallas_call x0 -> x2, Pallas kernels: none -> 205 us  [the longest x1 197 us: kernel_form(): pl.pallas_call(functools.partial(branch_kernel, n), out_shape=jax.ShapeDt...]
    dot_general x3 -> x0, matrix products: 43.7 us -> none  [the longest x1 23.4 us: on_device(): jnp.dot(hidden, lax.all_gather(down_weight, 'fs', axis=1, tiled=True), pr...]
    reduce_scatter x1 -> x0, waiting for transfers between devices: 42.9 us -> none  [on_device(): lax.psum_scatter(partials.astype(jnp.bfloat16), 'tp', scatter_dimension=0...]
    convert_element_type x5 -> x0, other arithmetic: 10.3 us -> none  [the longest x2 5.74 us: rounded(): lax.optimization_barrier(values.astype(jnp.bfloat16)).astype(jnp.float32)]
    unnamed x5 -> x0, local copies, waits for them, and re-layouts: 4.79 us -> none
  transfers between devices with their start and end apart: 5 -> 0, of which waited for: 5 -> 0; matrix products, arithmetic and copies ran while one was open for 7% -> 0% of each run, Pallas kernels for 0% -> 0%
where the time goes in v1:
time: 205 us
  Pallas kernels  205 us (100%)
    pallas_call x1, Pallas kernels, kernel_form(): pl.pallas_call(functools.partial(branch_kernel, n), out_shape=jax.ShapeDt...  197 us
    pallas_call x1, Pallas kernels, kernel_form(): pl.pallas_call(norm_kernel, grid=(rows // block,), out_shape=jax.ShapeDty...  7.39 us

profile of v1, /device:TPU:0, one launch (start us, length us, event | category | flops | bytes accessed | tf_op | source)
XLA Modules:
  0.0 204.8 jit_solution(502796206216194017)
XLA Ops:
  0.0 197.4 %branch.1.b_ref = bf16[1024,2048]{1,0:T(8,128)(2,1)} custom-call(bf16[1024,2048]{1,0:T(8,128)(2,1)} %t_ref.3, bf16[256,1408]{1,0:T(8,128)(2,1)} %g_ref.1, bf16[256,1408]{1,0:T(8,128)(2,1)} %v_ref.1, bf16[3,1408]{1,0:T(4,128)(2,1)} %gt_ref.1, bf16[3,1408]{1,0:T(4,128)(2,1)} %vt_ref.1, bf16[1408,256]{1,0:T(8,128)(2,1)} %d_ref.1), custom_call_target="tpu_custom_call" | custom-call | tf_op jit(solution)/shard_map/branch/pallas_call | solution.py:289
  197.5 7.4 %norm.1 = bf16[1024,2048]{1,0:T(8,128)(2,1)} custom-call(bf16[1024,2048]{1,0:T(8,128)(2,1)} %branch.1.b_ref, bf16[1024,2048]{1,0:T(8,128)(2,1)} %t_ref.3, f32[1,2048]{1,0:T(1,128)} %bitcast.2, f32[1,2048]{1,0:T(1,128)} %bitcast.3), custom_call_target="tpu_custom_call" | custom-call | tf_op jit(solution)/shard_map/norm/pallas_call | solution.py:323

commit v2 on v1

--- a/solution.py
+++ b/solution.py
@@ -58,9 +58,9 @@
 
 
 def branch_kernel(
-    n, t_ref, g_ref, v_ref, gt_ref, vt_ref, d_ref, out_ref,
-    gbuf, vbuf, dbuf, acc_g, acc_v, hid, pbuf, rbuf, cbuf, ybuf, obuf,
-    w_send, w_recv, c_send, c_recv, y_send, y_recv, o_send, o_recv,
+    n, t_hbm, g_ref, v_ref, gt_ref, vt_ref, d_ref, out_ref,
+    t_ref, gbuf, vbuf, dbuf, acc_g, acc_v, hid, pbuf, rbuf, cbuf, ybuf, obuf,
+    w_send, w_recv, c_send, c_recv, y_send, y_recv, o_send, o_recv, t_sem,
 ):
     rows, units = hid.shape
     half_rows = rows // 2
@@ -89,12 +89,15 @@
         )
     pl.semaphore_wait(barrier, 4)
 
-    streams = ((g_ref, gbuf), (v_ref, vbuf), (d_ref, dbuf))
+    streams = ((g_ref, gbuf), (v_ref, vbuf), (d_ref, dbuf), (d_ref, dbuf))
+    half_units = units // 2
 
     def hop(stream, way, step, first=False):
         own, slots = streams[stream]
         part = pl.ds(way * LANES, LANES)
-        where = (slice(None), part) if stream == 2 else (part, slice(None))
+        where = (part, slice(None))
+        if stream >= 2:
+            where = (pl.ds((stream - 2) * half_units, half_units), part)
         source = own.at[where] if first else slots.at[(step - 1,) + where]
         k = stream * 2 + way
         return pltpu.make_async_remote_copy(
@@ -120,6 +123,9 @@
 
     begin(0)
     begin(1)
+    load = pltpu.make_async_copy(t_hbm, t_ref, t_sem)
+    load.start()
+    load.wait()
 
     def token_tile(r, step):
         row = pl.ds(pl.multiple_of(r * tile, tile), tile)
@@ -137,16 +143,13 @@
 
     @pl.loop(1, n)
     def _(step):
-        @pl.when(step == n - 1)
-        def _():
-            arrive(2, 1)
-
         arrive(0, step)
         arrive(1, step)
 
-        @pl.when(step == n - 3)
+        @pl.when(step == n - 2)
         def _():
             begin(2)
+            begin(3)
 
         @pl.loop(0, rows // tile)
         def _(r):
@@ -172,7 +175,15 @@
         value = conv(acc_v, vt_ref, cols)
         hid[:, cols] = (gate / (1.0 + jnp.exp(-gate)) * value).astype(jnp.bfloat16)
 
+        @pl.when(i == chunks // 4)
+        def _():
+            arrive(2, 1)
+
         @pl.when(i == chunks // 2)
+        def _():
+            arrive(3, 1)
+
+        @pl.when(i == chunks - 2)
         def _():
             arrive(2, 2)
 
@@ -215,14 +226,19 @@
         )
 
     def project(step, weight):
-        @pl.loop(0, rows // tile)
-        def _(r):
-            row = pl.ds(pl.multiple_of(r * tile, tile), tile)
-            pbuf[step, row, :] = jnp.dot(
-                hid[row, :], weight, preferred_element_type=jnp.float32
-            ).astype(jnp.bfloat16)
-
+        def rows_from(first):
+            @pl.loop(0, half_rows // tile)
+            def _(r):
+                row = pl.ds(pl.multiple_of(first * half_rows + r * tile, tile), tile)
+                pbuf[step, row, :] = jnp.dot(
+                    hid[row, :], weight, preferred_element_type=jnp.float32
+                ).astype(jnp.bfloat16)
+
+        rows_from(1 - core)
         to_partner(step).start()
+        rows_from(core)
+
+    def pair(step):
         to_partner(step).wait_recv()
         cbuf[step] = (
             pbuf[step, mine].astype(jnp.float32) + rbuf[step].astype(jnp.float32)
@@ -240,25 +256,33 @@
             out_ref[mine, out_cols(step, way)] = total[:, way * LANES:(way + 1) * LANES]
 
     project(0, d_ref[...])
-
-    @pl.loop(1, n)
+    arrive(3, 2)
+    project(1, dbuf[0])
+    pair(0)
+
+    @pl.loop(2, n)
     def _(step):
         @pl.when(step > 2)
         def _():
             arrive(2, step)
 
+        pair(step - 1)
+
+        @pl.when(step > 2)
+        def _():
+            settle(step - 3)
+            arrive(3, step)
+
         project(step, dbuf[step - 1])
 
-        @pl.when(step >= 2)
-        def _():
-            settle(step - 2)
-
+    pair(n - 1)
+    settle(n - 3)
     settle(n - 2)
     settle(n - 1)
 
     @pl.loop(0, n - 1)
     def _(step):
-        for stream in range(3):
+        for stream in range(4):
             for way in range(2):
                 hop(stream, way, step, True).wait_send()
 
@@ -289,9 +313,11 @@
     branch = pl.pallas_call(
         functools.partial(branch_kernel, n),
         out_shape=jax.ShapeDtypeStruct((rows, width), bf16),
-        in_specs=[pl.BlockSpec(memory_space=pltpu.VMEM)] * 6,
+        in_specs=[pl.BlockSpec(memory_space=pl.ANY)]
+        + [pl.BlockSpec(memory_space=pltpu.VMEM)] * 5,
         out_specs=pl.BlockSpec(memory_space=pltpu.VMEM),
         scratch_shapes=[
+            pltpu.VMEM((rows, width), bf16),
             pltpu.VMEM((n - 1, depth, units), bf16),
             pltpu.VMEM((n - 1, depth, units), bf16),
             pltpu.VMEM((n - 1, units, depth), bf16),
@@ -303,14 +329,15 @@
             pltpu.VMEM((n, rows // 2, depth), bf16),
             pltpu.VMEM((n, rows // 2, depth), bf16),
             pltpu.VMEM((n, rows // 2, depth), bf16),
-            dma((6, n - 1)),
-            dma((6, n - 1)),
+            dma((8, n - 1)),
+            dma((8, n - 1)),
             dma((n,)),
             dma((n,)),
             dma((n,)),
             dma((n,)),
             dma((2, n)),
             dma((2, n)),
+            dma,
         ],
         compiler_params=pltpu.CompilerParams(
             collective_id=0, has_side_effects=True, vmem_limit_bytes=VMEM_BYTES

time: 205 us -> 191 us (0.932)
  Pallas kernels: 205 us -> 191 us
    pallas_call x1, Pallas kernels: 197 us -> 184 us  [kernel_form(): pl.pallas_call(functools.partial(branch_kernel, n), out_shape=jax.ShapeDt...]
where the time goes in v2:
time: 191 us
  Pallas kernels  191 us (100%)
    pallas_call x1, Pallas kernels, kernel_form(): pl.pallas_call(functools.partial(branch_kernel, n), out_shape=jax.ShapeDt...  184 us
    pallas_call x1, Pallas kernels, kernel_form(): pl.pallas_call(norm_kernel, grid=(rows // block,), out_shape=jax.ShapeDty...  7.39 us

profile of v2, /device:TPU:0, one launch (start us, length us, event | category | flops | bytes accessed | tf_op | source)
XLA Modules:
  0.0 191.1 jit_solution(2938207496457464768)
XLA Ops:
  0.0 183.7 %branch.1.b_ref = bf16[1024,2048]{1,0:T(8,128)(2,1)} custom-call(bf16[1024,2048]{1,0:T(8,128)(2,1)} %t_ref.1, bf16[256,1408]{1,0:T(8,128)(2,1)} %g_ref.1, bf16[256,1408]{1,0:T(8,128)(2,1)} %v_ref.1, bf16[3,1408]{1,0:T(4,128)(2,1)} %gt_ref.1, bf16[3,1408]{1,0:T(4,128)(2,1)} %vt_ref.1, bf16[1408,256]{1,0:T(8,128)(2,1)} %d_ref.1), custom_call_target="tpu_custom_call" | custom-call | tf_op jit(solution)/shard_map/branch/pallas_call | solution.py:313
  183.7 7.4 %norm.1 = bf16[1024,2048]{1,0:T(8,128)(2,1)} custom-call(bf16[1024,2048]{1,0:T(8,128)(2,1)} %branch.1.b_ref, bf16[1024,2048]{1,0:T(8,128)(2,1)} %t_ref.1, f32[1,2048]{1,0:T(1,128)} %bitcast.2, f32[1,2048]{1,0:T(1,128)} %bitcast.3), custom_call_target="tpu_custom_call" | custom-call | tf_op jit(solution)/shard_map/norm/pallas_call | solution.py:350

commit v3 on v2

--- a/solution.py
+++ b/solution.py
@@ -60,7 +60,7 @@
 def branch_kernel(
     n, t_hbm, g_ref, v_ref, gt_ref, vt_ref, d_ref, out_ref,
     t_ref, gbuf, vbuf, dbuf, acc_g, acc_v, hid, pbuf, rbuf, cbuf, ybuf, obuf,
-    w_send, w_recv, c_send, c_recv, y_send, y_recv, o_send, o_recv, t_sem,
+    w_send, w_recv, c_send, c_recv, y_send, y_recv, o_send, o_recv, l_sem, t_sem,
 ):
     rows, units = hid.shape
     half_rows = rows // 2
@@ -225,6 +225,13 @@
             device_id_type=pl.DeviceIdType.MESH,
         )
 
+    def to_own(step, way):
+        return pltpu.make_async_copy(
+            obuf.at[step, :, pl.ds(way * LANES, LANES)],
+            out_ref.at[mine, out_cols(step, way)],
+            l_sem.at[way, step],
+        )
+
     def project(step, weight):
         def rows_from(first):
             @pl.loop(0, half_rows // tile)
@@ -247,13 +254,12 @@
 
     def settle(step):
         to_across(step).wait_recv()
-        total = (
+        obuf[step] = (
             cbuf[step].astype(jnp.float32) + ybuf[step].astype(jnp.float32)
         ).astype(jnp.bfloat16)
-        obuf[step] = total
         for way in range(2):
             to_out(step, way, mine).start()
-            out_ref[mine, out_cols(step, way)] = total[:, way * LANES:(way + 1) * LANES]
+            to_own(step, way).start()
 
     project(0, d_ref[...])
     arrive(3, 2)
@@ -292,15 +298,50 @@
         to_across(step).wait_send()
         for way in range(2):
             to_out(step, way, mine).wait_send()
+            to_own(step, way).wait()
             to_out(step, way, other).wait_recv()
 
 
-def norm_kernel(b_ref, t_ref, gain_ref, bias_ref, out_ref):
-    mixed = RESIDUAL_SCALE * t_ref[...].astype(jnp.float32) + b_ref[...].astype(jnp.float32)
-    centered = mixed - jnp.mean(mixed, -1, keepdims=True)
-    variance = jnp.mean(centered * centered, -1, keepdims=True)
-    normed = centered * lax.rsqrt(variance + EPSILON) * gain_ref[...] + bias_ref[...]
-    out_ref[...] = normed.astype(jnp.bfloat16)
+NORM_ROWS = 128
+
+
+def norm_kernel(b_hbm, t_hbm, gain_ref, bias_ref, out_hbm, b_ref, t_ref, o_ref, in_sem, out_sem):
+    count = b_ref.shape[0] // NORM_ROWS
+
+    def chunk(i):
+        return pl.ds(pl.multiple_of(i * NORM_ROWS, NORM_ROWS), NORM_ROWS)
+
+    def loads(i):
+        part = chunk(i)
+        return (
+            pltpu.make_async_copy(b_hbm.at[part], b_ref.at[part], in_sem.at[0, i]),
+            pltpu.make_async_copy(t_hbm.at[part], t_ref.at[part], in_sem.at[1, i]),
+        )
+
+    def store(i):
+        part = chunk(i)
+        return pltpu.make_async_copy(o_ref.at[part], out_hbm.at[part], out_sem.at[i])
+
+    for i in range(count):
+        for load in loads(i):
+            load.start()
+
+    @pl.loop(0, count)
+    def _(i):
+        for load in loads(i):
+            load.wait()
+        part = chunk(i)
+        mixed = RESIDUAL_SCALE * t_ref[part, :].astype(jnp.float32)
+        mixed += b_ref[part, :].astype(jnp.float32)
+        centered = mixed - jnp.mean(mixed, -1, keepdims=True)
+        variance = jnp.mean(centered * centered, -1, keepdims=True)
+        normed = centered * lax.rsqrt(variance + EPSILON) * gain_ref[...] + bias_ref[...]
+        o_ref[part, :] = normed.astype(jnp.bfloat16)
+        store(i).start()
+
+    @pl.loop(0, count)
+    def _(i):
+        store(i).wait()
 
 
 def kernel_form(
@@ -315,7 +356,7 @@
         out_shape=jax.ShapeDtypeStruct((rows, width), bf16),
         in_specs=[pl.BlockSpec(memory_space=pl.ANY)]
         + [pl.BlockSpec(memory_space=pltpu.VMEM)] * 5,
-        out_specs=pl.BlockSpec(memory_space=pltpu.VMEM),
+        out_specs=pl.BlockSpec(memory_space=pl.ANY),
         scratch_shapes=[
             pltpu.VMEM((rows, width), bf16),
             pltpu.VMEM((n - 1, depth, units), bf16),
@@ -337,6 +378,7 @@
             dma((n,)),
             dma((2, n)),
             dma((2, n)),
+            dma((2, n)),
             dma,
         ],
         compiler_params=pltpu.CompilerParams(
@@ -344,15 +386,16 @@
         ),
         name="branch",
     )(tokens, gate_weight, value_weight, gate_taps, value_taps, down_weight)
-    block = 256
-    by_rows = pl.BlockSpec((block, width), lambda i: (i, 0))
-    whole = pl.BlockSpec((1, width), lambda i: (0, 0))
+    anywhere = pl.BlockSpec(memory_space=pl.ANY)
+    vector = pl.BlockSpec(memory_space=pltpu.VMEM)
+    count = rows // NORM_ROWS
     return pl.pallas_call(
         norm_kernel,
-        grid=(rows // block,),
         out_shape=jax.ShapeDtypeStruct((rows, width), bf16),
-        in_specs=[by_rows, by_rows, whole, whole],
-        out_specs=by_rows,
+        in_specs=[anywhere, anywhere, vector, vector],
+        out_specs=anywhere,
+        scratch_shapes=[pltpu.VMEM((rows, width), bf16)] * 3 + [dma((2, count)), dma((count,))],
+        compiler_params=pltpu.CompilerParams(vmem_limit_bytes=VMEM_BYTES),
         name="norm",
     )(branch, tokens, norm_gain.reshape(1, width), norm_bias.reshape(1, width))
 

time: 191 us -> 189 us (0.990)
  Pallas kernels: 191 us -> 189 us
where the time goes in v3:
time: 189 us
  Pallas kernels  189 us (100%)
    pallas_call x1, Pallas kernels, kernel_form(): pl.pallas_call(functools.partial(branch_kernel, n), out_shape=jax.ShapeDt...  182 us
    pallas_call x1, Pallas kernels, kernel_form(): pl.pallas_call(norm_kernel, out_shape=jax.ShapeDtypeStruct((rows, width),...  6.53 us

profile of v3, /device:TPU:0, one launch (start us, length us, event | category | flops | bytes accessed | tf_op | source)
XLA Modules:
  0.0 188.6 jit_solution(17448475739033729587)
XLA Ops:
  0.0 182.0 %branch.1.b_hbm = bf16[1024,2048]{1,0:T(8,128)(2,1)} custom-call(bf16[1024,2048]{1,0:T(8,128)(2,1)} %t_hbm.3, bf16[256,1408]{1,0:T(8,128)(2,1)} %g_ref.1, bf16[256,1408]{1,0:T(8,128)(2,1)} %v_ref.1, bf16[3,1408]{1,0:T(4,128)(2,1)} %gt_ref.1, bf16[3,1408]{1,0:T(4,128)(2,1)} %vt_ref.1, bf16[1408,256]{1,0:T(8,128)(2,1)} %d_ref.1), custom_call_target="tpu_custom_call" | custom-call | tf_op jit(solution)/shard_map/branch/pallas_call | solution.py:354
  182.0 6.5 %norm.1 = bf16[1024,2048]{1,0:T(8,128)(2,1)} custom-call(bf16[1024,2048]{1,0:T(8,128)(2,1)} %branch.1.b_hbm, bf16[1024,2048]{1,0:T(8,128)(2,1)} %t_hbm.3, f32[1,2048]{1,0:T(1,128)} %bitcast.2, f32[1,2048]{1,0:T(1,128)} %bitcast.3), custom_call_target="tpu_custom_call" | custom-call | tf_op jit(solution)/shard_map/norm/pallas_call | solution.py:392

commit v4 on v3

--- a/solution.py
+++ b/solution.py
@@ -58,8 +58,8 @@
 
 
 def branch_kernel(
-    n, t_hbm, g_ref, v_ref, gt_ref, vt_ref, d_ref, out_ref,
-    t_ref, gbuf, vbuf, dbuf, acc_g, acc_v, hid, pbuf, rbuf, cbuf, ybuf, obuf,
+    n, t_hbm, g_hbm, v_hbm, gt_ref, vt_ref, d_hbm, out_ref,
+    t_ref, g_ref, v_ref, d_ref, gbuf, vbuf, dbuf, acc_g, acc_v, hid, pbuf, rbuf, cbuf, ybuf, obuf,
     w_send, w_recv, c_send, c_recv, y_send, y_recv, o_send, o_recv, l_sem, t_sem,
 ):
     rows, units = hid.shape
@@ -81,6 +81,11 @@
         return (1 - down) * 2 * p + down * (2 * (n - 1 - p) + 1)
 
     right, left = at_pos(pos + 1), at_pos(pos + n - 1)
+
+    pairs = ((g_hbm, g_ref), (v_hbm, v_ref), (t_hbm, t_ref), (d_hbm, d_ref))
+    loads = [pltpu.make_async_copy(a, b, t_sem.at[i]) for i, (a, b) in enumerate(pairs)]
+    for load in loads:
+        load.start()
 
     barrier = pltpu.get_barrier_semaphore()
     for target in ({"fs": left}, {"fs": right}, {"tp": partner}, {"tp": across}):
@@ -121,11 +126,12 @@
             def _():
                 hop(stream, way, step).start()
 
+    loads[0].wait()
     begin(0)
+    loads[1].wait()
     begin(1)
-    load = pltpu.make_async_copy(t_hbm, t_ref, t_sem)
-    load.start()
-    load.wait()
+    loads[2].wait()
+    loads[3].wait()
 
     def token_tile(r, step):
         row = pl.ds(pl.multiple_of(r * tile, tile), tile)
@@ -351,14 +357,18 @@
     depth, units = gate_weight.shape
     bf16, f32 = jnp.bfloat16, jnp.float32
     dma = pltpu.SemaphoreType.DMA
+    anywhere = pl.BlockSpec(memory_space=pl.ANY)
+    vector = pl.BlockSpec(memory_space=pltpu.VMEM)
     branch = pl.pallas_call(
         functools.partial(branch_kernel, n),
         out_shape=jax.ShapeDtypeStruct((rows, width), bf16),
-        in_specs=[pl.BlockSpec(memory_space=pl.ANY)]
-        + [pl.BlockSpec(memory_space=pltpu.VMEM)] * 5,
+        in_specs=[anywhere] * 3 + [vector] * 2 + [anywhere],
         out_specs=pl.BlockSpec(memory_space=pl.ANY),
         scratch_shapes=[
             pltpu.VMEM((rows, width), bf16),
+            pltpu.VMEM((depth, units), bf16),
+            pltpu.VMEM((depth, units), bf16),
+            pltpu.VMEM((units, depth), bf16),
             pltpu.VMEM((n - 1, depth, units), bf16),
             pltpu.VMEM((n - 1, depth, units), bf16),
             pltpu.VMEM((n - 1, units, depth), bf16),
@@ -379,15 +389,13 @@
             dma((2, n)),
             dma((2, n)),
             dma((2, n)),
-            dma,
+            dma((4,)),
         ],
         compiler_params=pltpu.CompilerParams(
             collective_id=0, has_side_effects=True, vmem_limit_bytes=VMEM_BYTES
         ),
         name="branch",
     )(tokens, gate_weight, value_weight, gate_taps, value_taps, down_weight)
-    anywhere = pl.BlockSpec(memory_space=pl.ANY)
-    vector = pl.BlockSpec(memory_space=pltpu.VMEM)
     count = rows // NORM_ROWS
     return pl.pallas_call(
         norm_kernel,

time: 189 us -> 188 us (level)
  no operation moved by 1% of the time
where the time goes in v4:
time: 188 us
  Pallas kernels  188 us (100%)
    pallas_call x1, Pallas kernels, kernel_form(): pl.pallas_call(functools.partial(branch_kernel, n), out_shape=jax.ShapeDt...  181 us
    pallas_call x1, Pallas kernels, kernel_form(): pl.pallas_call(norm_kernel, out_shape=jax.ShapeDtypeStruct((rows, width),...  6.53 us

profile of v4, /device:TPU:0, one launch (start us, length us, event | category | flops | bytes accessed | tf_op | source)
XLA Modules:
  0.0 187.7 jit_solution(18165109148129141078)
XLA Ops:
  0.0 181.2 %branch.1.b_hbm = bf16[1024,2048]{1,0:T(8,128)(2,1)} custom-call(bf16[1024,2048]{1,0:T(8,128)(2,1)} %t_hbm.3, bf16[256,1408]{1,0:T(8,128)(2,1)} %g_hbm.1, bf16[256,1408]{1,0:T(8,128)(2,1)} %v_hbm.1, bf16[3,1408]{1,0:T(4,128)(2,1)} %gt_ref.1, bf16[3,1408]{1,0:T(4,128)(2,1)} %vt_ref.1, bf16[1408,256]{1,0:T(8,128)(2,1)} %d_hbm.1), custom_call_target="tpu_custom_call" | custom-call | tf_op jit(solution)/shard_map/branch/pallas_call | solution.py:362
  181.2 6.5 %norm.1 = bf16[1024,2048]{1,0:T(8,128)(2,1)} custom-call(bf16[1024,2048]{1,0:T(8,128)(2,1)} %branch.1.b_hbm, bf16[1024,2048]{1,0:T(8,128)(2,1)} %t_hbm.3, f32[1,2048]{1,0:T(1,128)} %bitcast.2, f32[1,2048]{1,0:T(1,128)} %bitcast.3), custom_call_target="tpu_custom_call" | custom-call | tf_op jit(solution)/shard_map/norm/pallas_call | solution.py:400
